TPU v7x, 32 devices: a whole 2x2x4 slice. The times are simulated.
32 devices in a mesh: sp: 16 (over z, y, x), tp: 2 (over core).
Axes of the slice: x: 2, y: 2, z: 4, core: 2. Of those that a mesh axis runs over, the one named last changes fastest.
Arguments:
- queries: bfloat16 [4096, 1024], P('sp', 'tp'), may hold values from -6 to 6
- keys: bfloat16 [4096, 1024], P('sp', 'tp'), may hold values from -6 to 6
- values: bfloat16 [4096, 1024], P('sp', 'tp'), may hold values from -6 to 6
- lambdas: float32 [8], P('tp'), may hold values from 0.3 to 0.8
- head_gain: float32 [128], replicated, may hold values from 0.1 to 1.9
- out_weight: bfloat16 [1024, 2048], P('tp'), may hold values from -0.1875 to 0.1875
- residual: bfloat16 [4096, 2048], P(('sp', 'tp')), may hold values from -6 to 6
- mix_gain: float32 [2048], replicated, may hold values from 0.1 to 1.9
- pre_gain: float32 [2048], replicated, may hold values from 0.1 to 1.9
- gate_weight: bfloat16 [2048, 2816], P('sp', 'tp'), may hold values from -0.125 to 0.125
- up_weight: bfloat16 [2048, 2816], P('sp', 'tp'), may hold values from -0.125 to 0.125
- down_weight: bfloat16 [2048, 2816], P('sp', 'tp'), may hold values from -0.109375 to 0.109375
- ffn_gain: float32 [2048], replicated, may hold values from 0.1 to 1.9
Outputs:
- result: bfloat16 [4096, 2048], P(('sp', 'tp'))
All inputs are finite; a program needn't handle non-finite values.
Results may differ from a plain program's by a relative error of at most 0.02.
Values may be sent and summed in bfloat16 or wider, within the bound.
A program may use at most 64 MiB of HBM per device.

v0:
```python
import math

import jax
import jax.numpy as jnp
from jax import lax
from jax.sharding import PartitionSpec as P

KD = 64
VD = 128


epsilon = 1e-06
negative = -1e30


def normalize(matrix, gain):
    return matrix * lax.rsqrt(jnp.mean(matrix * matrix, axis=-1, keepdims=True) + epsilon) * gain


def rounded(matrix):
    return lax.optimization_barrier(matrix.astype(jnp.bfloat16)).astype(jnp.float32)


def on_device(
    queries,
    keys,
    values,
    lambdas,
    head_gain,
    out_weight,
    residual,
    mix_gain,
    pre_gain,
    gate_weight,
    up_weight,
    down_weight,
    ffn_gain,
):
    rows = queries.shape[0]
    heads_dev = values.shape[1] // VD
    offset = lax.axis_index("sp") * rows
    scale = 1.0 / math.sqrt(KD)
    groups = [(queries, offset + jnp.arange(rows, dtype=jnp.int32))]
    grids = [
        (group_rows.reshape(group_rows.shape[0], heads_dev, 2, KD), group_pos)
        for group_rows, group_pos in groups
    ]
    initial = tuple(
        (
            (
                jnp.full((heads_dev, 2, grid.shape[0]), negative, jnp.float32),
                jnp.zeros((heads_dev, 2, grid.shape[0]), jnp.float32),
                jnp.zeros((heads_dev, 2, grid.shape[0], VD), jnp.float32),
            )
            for grid, _ in grids
        )
    )
    key_piece = lax.all_gather(keys, "sp", axis=0, tiled=True)
    value_piece = lax.all_gather(values, "sp", axis=0, tiled=True)
    count = key_piece.shape[0]
    block = math.gcd(count, max(256, 2048 // heads_dev))
    key_grid = key_piece.reshape(count, heads_dev, 2, KD)
    value_grid = value_piece.reshape(count, heads_dev, VD)
    results = []
    for (query_grid, query_pos), carried_group in zip(grids, initial):
        last_pos = query_pos[-1]

        def visit(index, carried, query_grid=query_grid, query_pos=query_pos, last_pos=last_pos):
            first = index * block

            def update(current):
                maxima, totals, accum = current
                key_block = lax.dynamic_slice_in_dim(key_grid, first, block, 0)
                value_block = lax.dynamic_slice_in_dim(value_grid, first, block, 0)
                scores = (
                    jnp.einsum(
                        "rhcd,nhcd->hcrn", query_grid, key_block, preferred_element_type=jnp.float32
                    )
                    * scale
                )
                key_pos = first + jnp.arange(block, dtype=jnp.int32)
                visible = key_pos[None, :] <= query_pos[:, None]
                block_max = jnp.max(jnp.where(visible, scores, negative), axis=-1)
                new_max = jnp.maximum(maxima, block_max)
                weights = jnp.where(visible, jnp.exp(scores - new_max[..., None]), 0.0)
                factor = jnp.exp(maxima - new_max)
                totals = totals * factor + jnp.sum(weights, axis=-1)
                accum = accum * factor[..., None] + jnp.einsum(
                    "hcrn,nhe->hcre",
                    weights.astype(jnp.bfloat16),
                    value_block,
                    preferred_element_type=jnp.float32,
                )
                return (new_max, totals, accum)

            return lax.cond(first <= last_pos, update, lambda current: current, carried)

        results.append(lax.fori_loop(0, count // block, visit, carried_group))
    states = tuple(results)
    totals = jnp.concatenate([state[1] for state in states], axis=2)
    accum = jnp.concatenate([state[2] for state in states], axis=2)
    ratio = accum / totals[..., None]
    attended = ratio[:, 0] - lambdas[:, None, None] * ratio[:, 1]
    heads_normed = normalize(attended, head_gain).astype(jnp.bfloat16)
    head_out = jnp.transpose(heads_normed, (1, 0, 2)).reshape(rows, heads_dev * VD)
    section = head_out
    projected = lax.psum_scatter(
        rounded(jnp.dot(section, out_weight, preferred_element_type=jnp.float32)).astype(
            jnp.bfloat16
        ),
        "tp",
        scatter_dimension=0,
        tiled=True,
    ).astype(jnp.float32)
    mixed = (residual.astype(jnp.float32) + normalize(projected, mix_gain)).astype(jnp.bfloat16)
    normed = normalize(mixed.astype(jnp.float32), pre_gain).astype(jnp.bfloat16)
    inputs = lax.all_gather(normed, "tp", axis=0, tiled=True)
    gate_sum = jnp.dot(
        inputs,
        lax.all_gather(gate_weight, "sp", axis=0, tiled=True),
        preferred_element_type=jnp.float32,
    )
    up_sum = jnp.dot(
        inputs,
        lax.all_gather(up_weight, "sp", axis=0, tiled=True),
        preferred_element_type=jnp.float32,
    )
    down_rows = lax.all_gather(down_weight, "sp", axis=0, tiled=True)
    hidden = (jax.nn.silu(gate_sum) * up_sum).astype(jnp.bfloat16)
    section = hidden
    ffn_out = lax.psum_scatter(
        rounded(
            lax.dot_general(
                section, down_rows, (((1,), (1,)), ((), ())), preferred_element_type=jnp.float32
            )
        ).astype(jnp.bfloat16),
        "tp",
        scatter_dimension=0,
        tiled=True,
    ).astype(jnp.float32)
    return (mixed.astype(jnp.float32) + normalize(ffn_out, ffn_gain)).astype(jnp.bfloat16)


def solution(mesh):
    in_specs = (
        P("sp", "tp"),
        P("sp", "tp"),
        P("sp", "tp"),
        P("tp"),
        P(),
        P("tp", None),
        P(("sp", "tp"), None),
        P(),
        P(),
        P("sp", "tp"),
        P("sp", "tp"),
        P("sp", "tp"),
        P(),
    )
    out_specs = P(("sp", "tp"), None)
    return jax.shard_map(
        on_device, mesh=mesh, in_specs=in_specs, out_specs=out_specs, check_vma=False
    )
```

profile of v0, /device:TPU:25, one launch (start us, length us, event | category | flops | bytes accessed | tf_op | source)
XLA Modules:
  0.0 555.5 jit_solution(14109540830264197258)
XLA Ops:
  6.5 1.9 copy.21
  8.6 0.7 all-gather.7.cloned.1.call-update
  9.3 0.7 slice.9
  10.0 1.1 copy.20
  11.1 83.9 %all-gather.9.cloned.1.call-done = bf16[4096,512]{0,1:T(8,128)(2,1)} async-done(((bf16[256,512]{0,1:T(8,128)(2,1)}), bf16[4096,512]{0,1:T(8,128)(2,1)}) %all-gather.9.cloned.1.call-update) | async-done | bytes 4194320 | tf_op jit(solution)/shard_map/all_gather | solution.py:59
  94.9 6.3 %copy.22 = bf16[4096,4,128]{2,0,1:T(8,128)(2,1)} copy(bf16[4096,4,128]{0,2,1:T(8,128)(2,1)} %bitcast.62) | data formatting | bytes 8388608
  101.3 71.0 %all-gather.7.cloned.1.call-done = bf16[4096,512]{1,0:T(8,128)(2,1)} async-done(((bf16[256,512]{1,0:T(8,128)(2,1)}), bf16[4096,512]{1,0:T(8,128)(2,1)}) %all-gather.7.cloned.1.call-update) | async-done | bytes 4194320 | tf_op jit(solution)/shard_map/all_gather | solution.py:58
  172.3 6.5 %copy.19 = bf16[4096,512]{0,1:T(8,128)(2,1)} copy(bf16[4096,512]{1,0:T(8,128)(2,1)} %all-gather.7.cloned.1.call-done) | data formatting | bytes 8388608 | tf_op jit(solution)/shard_map/all_gather | solution.py:58
  178.9 45.0 %while.18 = (s32[]{:T(128)}, f32[4,2,256]{2,1,0:T(2,128)S(1)}, f32[4,2,256]{2,1,0:T(2,128)S(1)}, f32[4,2,256,128]{3,2,1,0:T(8,128)S(1)}, s32[]{:T(128)}, /*index...) while((s32[]{:T(128)}, f32[4,2,256]{2,1,0:T(2,128)S(1)}, ...), condition=%wide.region_5.6_spmd.clone, body=%wide.region_0.5_spmd.clone.sunk | while | flops 414847744 | bytes 16654649 | solution.py:98
  179.6 5.6 %conditional.3 = ((f32[4,2,256]{2,1,0:T(2,128)S(1)}, f32[4,2,256]{2,1,0:T(2,128)S(1)}, f32[4,2,256,128]{3,2,1,0:T(8,128)S(1)})) conditional(s32[]{:T(128)} %convert_element_type.109, (f32[4,2,256]{2,1,0:T(2,128)S(1)}, f32[4,2,256]{2,1,0:T(2,128)S(1)}, f32[4,2,256,128]{3,2,1,0:T(8,128)S(1)}) %tuple.47, (s32[]{:T(128)}, s32[]{:T(128)}, ...), branch_computations={%region_1.0_spmd, %region_2.4_spmd} | conditional | flops 414847744 | bytes 16653394 | solution.py:96
  179.6 0.1 broadcast_compare_fusion
  179.8 1.9 fusion.2
  181.7 0.9 fusion.6
  182.6 2.6 fusion.13
  185.9 5.6 %conditional.3 = ((f32[4,2,256]{2,1,0:T(2,128)S(1)}, f32[4,2,256]{2,1,0:T(2,128)S(1)}, f32[4,2,256,128]{3,2,1,0:T(8,128)S(1)})) conditional(s32[]{:T(128)} %convert_element_type.109, (f32[4,2,256]{2,1,0:T(2,128)S(1)}, f32[4,2,256]{2,1,0:T(2,128)S(1)}, f32[4,2,256,128]{3,2,1,0:T(8,128)S(1)}) %tuple.47, (s32[]{:T(128)}, s32[]{:T(128)}, ...), branch_computations={%region_1.0_spmd, %region_2.4_spmd} | conditional | flops 414847744 | bytes 16653394 | solution.py:96
  186.0 0.1 broadcast_compare_fusion
  186.1 1.9 fusion.2
  188.0 0.9 fusion.6
  188.9 2.6 fusion.13
  192.2 5.6 %conditional.3 = ((f32[4,2,256]{2,1,0:T(2,128)S(1)}, f32[4,2,256]{2,1,0:T(2,128)S(1)}, f32[4,2,256,128]{3,2,1,0:T(8,128)S(1)})) conditional(s32[]{:T(128)} %convert_element_type.109, (f32[4,2,256]{2,1,0:T(2,128)S(1)}, f32[4,2,256]{2,1,0:T(2,128)S(1)}, f32[4,2,256,128]{3,2,1,0:T(8,128)S(1)}) %tuple.47, (s32[]{:T(128)}, s32[]{:T(128)}, ...), branch_computations={%region_1.0_spmd, %region_2.4_spmd} | conditional | flops 414847744 | bytes 16653394 | solution.py:96
  192.3 0.1 broadcast_compare_fusion
  192.4 1.9 fusion.2
  194.3 0.9 fusion.6
  195.2 2.6 fusion.13
  198.6 5.6 %conditional.3 = ((f32[4,2,256]{2,1,0:T(2,128)S(1)}, f32[4,2,256]{2,1,0:T(2,128)S(1)}, f32[4,2,256,128]{3,2,1,0:T(8,128)S(1)})) conditional(s32[]{:T(128)} %convert_element_type.109, (f32[4,2,256]{2,1,0:T(2,128)S(1)}, f32[4,2,256]{2,1,0:T(2,128)S(1)}, f32[4,2,256,128]{3,2,1,0:T(8,128)S(1)}) %tuple.47, (s32[]{:T(128)}, s32[]{:T(128)}, ...), branch_computations={%region_1.0_spmd, %region_2.4_spmd} | conditional | flops 414847744 | bytes 16653394 | solution.py:96
  198.6 0.1 broadcast_compare_fusion
  198.7 1.9 fusion.2
  200.7 0.9 fusion.6
  201.6 2.6 fusion.13
  204.9 5.6 %conditional.3 = ((f32[4,2,256]{2,1,0:T(2,128)S(1)}, f32[4,2,256]{2,1,0:T(2,128)S(1)}, f32[4,2,256,128]{3,2,1,0:T(8,128)S(1)})) conditional(s32[]{:T(128)} %convert_element_type.109, (f32[4,2,256]{2,1,0:T(2,128)S(1)}, f32[4,2,256]{2,1,0:T(2,128)S(1)}, f32[4,2,256,128]{3,2,1,0:T(8,128)S(1)}) %tuple.47, (s32[]{:T(128)}, s32[]{:T(128)}, ...), branch_computations={%region_1.0_spmd, %region_2.4_spmd} | conditional | flops 414847744 | bytes 16653394 | solution.py:96
  204.9 0.1 broadcast_compare_fusion
  205.1 1.9 fusion.2
  207.0 0.9 fusion.6
  207.9 2.6 fusion.13
  211.2 5.6 %conditional.3 = ((f32[4,2,256]{2,1,0:T(2,128)S(1)}, f32[4,2,256]{2,1,0:T(2,128)S(1)}, f32[4,2,256,128]{3,2,1,0:T(8,128)S(1)})) conditional(s32[]{:T(128)} %convert_element_type.109, (f32[4,2,256]{2,1,0:T(2,128)S(1)}, f32[4,2,256]{2,1,0:T(2,128)S(1)}, f32[4,2,256,128]{3,2,1,0:T(8,128)S(1)}) %tuple.47, (s32[]{:T(128)}, s32[]{:T(128)}, ...), branch_computations={%region_1.0_spmd, %region_2.4_spmd} | conditional | flops 414847744 | bytes 16653394 | solution.py:96
  211.3 0.1 broadcast_compare_fusion
  211.4 1.9 fusion.2
  213.3 0.9 fusion.6
  214.2 2.6 fusion.13
  217.5 5.6 %conditional.3 = ((f32[4,2,256]{2,1,0:T(2,128)S(1)}, f32[4,2,256]{2,1,0:T(2,128)S(1)}, f32[4,2,256,128]{3,2,1,0:T(8,128)S(1)})) conditional(s32[]{:T(128)} %convert_element_type.109, (f32[4,2,256]{2,1,0:T(2,128)S(1)}, f32[4,2,256]{2,1,0:T(2,128)S(1)}, f32[4,2,256,128]{3,2,1,0:T(8,128)S(1)}) %tuple.47, (s32[]{:T(128)}, s32[]{:T(128)}, ...), branch_computations={%region_1.0_spmd, %region_2.4_spmd} | conditional | flops 414847744 | bytes 16653394 | solution.py:96
  217.7 1.9 fusion.2
  219.6 0.9 fusion.6
  220.5 2.6 fusion.13
  223.9 1.3 copy.24
  225.2 1.3 broadcast_divide_fusion
  226.6 0.2 multiply_reduce_fusion
  226.8 0.1 multiply_convert_fusion
  227.0 1.7 convolution_convert_fusion
  228.7 0.5 all-gather.13.cloned.1.call-update
  229.3 15.0 %reduce-scatter.3.cloned.1.call-done = bf16[128,2048]{1,0:T(8,128)(2,1)} async-done(((bf16[256,2048]{1,0:T(8,128)(2,1)}), bf16[128,2048]{1,0:T(8,128)(2,1)}) %reduce-scatter.3.cloned.1.call-update) | async-done | bytes 524304 | tf_op jit(solution)/shard_map/reduce_scatter | solution.py:107
  244.3 1.2 fusion.25
  245.5 1.4 fusion.31
  247.0 1.0 fusion.33
  248.1 0.5 all-gather.15.cloned.1.call-update
  248.6 0.7 all-gather.17.cloned.1.call-update
  249.4 85.3 %all-gather.13.cloned.1.call-done = bf16[2048,1408]{1,0:T(8,128)(2,1)} async-done(((bf16[128,1408]{1,0:T(8,128)(2,1)}), bf16[2048,1408]{1,0:T(8,128)(2,1)}) %all-gather.13.cloned.1.call-update) | async-done | bytes 5767184 | tf_op jit(solution)/shard_map/all_gather | solution.py:120
  334.6 11.3 %all-gather.11.cloned.1.call-done = bf16[256,2048]{1,0:T(8,128)(2,1)} async-done(((bf16[128,2048]{1,0:T(8,128)(2,1)}), bf16[256,2048]{1,0:T(8,128)(2,1)}) %all-gather.11.cloned.1.call-update) | async-done | bytes 1048592 | tf_op jit(solution)/shard_map/all_gather | solution.py:117
  346.0 5.9 %fusion.39 = f32[256,1408]{1,0:T(8,128)} fusion(bf16[256,2048]{1,0:T(8,128)(2,1)} %all-gather.11.cloned.1.call-done, bf16[2048,1408]{1,0:T(8,128)(2,1)} %all-gather.13.cloned.1.call-done), kind=kOutput, calls=%fused_computation.61 | convolution fusion | flops 1476395008 | bytes 8257536 | tf_op jit(solution)/shard_map/dot_general | solution.py:118
  351.9 84.4 %all-gather.15.cloned.1.call-done = bf16[2048,1408]{1,0:T(8,128)(2,1)} async-done(((bf16[128,1408]{1,0:T(8,128)(2,1)}), bf16[2048,1408]{1,0:T(8,128)(2,1)}) %all-gather.15.cloned.1.call-update) | async-done | bytes 5767184 | tf_op jit(solution)/shard_map/all_gather | solution.py:125
  436.3 90.1 %all-gather.17.cloned.1.call-done = bf16[2048,1408]{1,0:T(8,128)(2,1)} async-done(((bf16[128,1408]{1,0:T(8,128)(2,1)}), bf16[2048,1408]{1,0:T(8,128)(2,1)}) %all-gather.17.cloned.1.call-update) | async-done | bytes 5767184 | tf_op jit(solution)/shard_map/all_gather | solution.py:128
  526.4 9.5 %convolution_convert_fusion.1 = bf16[256,2048]{1,0:T(8,128)(2,1)} fusion(bf16[2048,1408]{1,0:T(8,128)(2,1)} %all-gather.17.cloned.1.call-done, bf16[256,2048]{1,0:T(8,128)(2,1)} %all-gather.11.cloned.1.call-done, bf16[2048,1408]{1,0:T(8,128)(2,1)} %all-gather.15.cloned.1.call-done, f32[256,1408]{1,0:T(8,128)} %fusion.39), kind=kOutput, calls=%fused_computation.30 | convolution fusion | flops 2955476992 | bytes 15073280 | tf_op jit(solution)/shard_map/dot_general | solution.py:133
  535.9 9.4 %reduce-scatter.5.cloned.1.call-done = bf16[128,2048]{1,0:T(8,128)(2,1)} async-done(((bf16[256,2048]{1,0:T(8,128)(2,1)}), bf16[128,2048]{1,0:T(8,128)(2,1)}) %reduce-scatter.5.cloned.1.call-update) | async-done | bytes 524304 | tf_op jit(solution)/shard_map/reduce_scatter | solution.py:131
  545.3 1.2 fusion.29
  546.6 2.1 fusion.34
  (80 shorter events, 0.9 us)
Async XLA Ops:
  6.5 220.4 %copy-start = (bf16[512,2048]{1,0:T(8,128)(2,1)S(1)}, bf16[512,2048]{1,0:T(8,128)(2,1)}, u32[]{:S(2)}) copy-start(bf16[512,2048]{1,0:T(8,128)(2,1)} %param.22) | copy-start | bytes 6291460
  6.5 88.4 %all-gather.9.cloned.1.call-start = ((), (), s32[]{:S(2)}) async-start(), calls=%async_computation.3 | async-start | bytes 4456448 | tf_op jit(solution)/shard_map/all_gather | solution.py:59
  8.5 163.8 %all-gather.7.cloned.1.call-start = ((), (), s32[]{:S(2)}) async-start(), calls=%async_computation.2 | async-start | bytes 4456448 | tf_op jit(solution)/shard_map/all_gather | solution.py:58
  9.3 235.0 %reduce-scatter.3.cloned.1.call-start = ((), (), s32[]{:S(2)}) async-start(), calls=%async_computation.4 | async-start | bytes 1572864 | tf_op jit(solution)/shard_map/reduce_scatter | solution.py:107
  223.9 2.7 copy-start.5
  223.9 2.9 copy-start.6
  226.6 18.9 %copy-start.1 = (bf16[128,2048]{1,0:T(8,128)(2,1)S(1)}, bf16[128,2048]{1,0:T(8,128)(2,1)}, u32[]{:S(2)}) copy-start(bf16[128,2048]{1,0:T(8,128)(2,1)} %param.23) | copy-start | bytes 1572868
  226.6 18.9 %copy-start.2 = (f32[2048]{0:T(1024)S(1)}, f32[2048]{0:T(1024)}, u32[]{:S(2)}) copy-start(f32[2048]{0:T(1024)} %param.24) | copy-start | bytes 24580
  226.8 20.2 %copy-start.3 = (f32[2048]{0:T(1024)S(1)}, f32[2048]{0:T(1024)}, u32[]{:S(2)}) copy-start(f32[2048]{0:T(1024)} %param.25) | copy-start | bytes 24580
  228.7 105.9 %all-gather.13.cloned.1.call-start = ((), (), s32[]{:S(2)}) async-start(), calls=%async_computation.6 | async-start | bytes 6127616 | tf_op jit(solution)/shard_map/all_gather | solution.py:120
  229.3 116.7 %all-gather.11.cloned.1.call-start = ((), (), s32[]{:S(2)}) async-start(), calls=%async_computation.5 | async-start | bytes 1572864 | tf_op jit(solution)/shard_map/all_gather | solution.py:117
  248.0 188.3 %all-gather.15.cloned.1.call-start = ((), (), s32[]{:S(2)}) async-start(), calls=%async_computation.7 | async-start | bytes 6127616 | tf_op jit(solution)/shard_map/all_gather | solution.py:125
  248.6 277.8 %all-gather.17.cloned.1.call-start = ((), (), s32[]{:S(2)}) async-start(), calls=%async_computation.8 | async-start | bytes 6127616 | tf_op jit(solution)/shard_map/all_gather | solution.py:128
  249.3 296.0 %reduce-scatter.5.cloned.1.call-start = ((), (), s32[]{:S(2)}) async-start(), calls=%async_computation.9 | async-start | bytes 1572864 | tf_op jit(solution)/shard_map/reduce_scatter | solution.py:131
  351.9 194.7 %copy-start.4 = (f32[2048]{0:T(1024)S(1)}, f32[2048]{0:T(1024)}, u32[]{:S(2)}) copy-start(f32[2048]{0:T(1024)} %param.29) | copy-start | bytes 24580
Sparse Core Ops, SparseCore 0:
  10.1 84.8 all-gather.8
  97.7 74.4 all-gather.6
  228.8 15.4 reduce-scatter.2
  246.8 87.7 all-gather.12
  336.0 9.8 all-gather.10
  348.5 87.7 all-gather.14
  439.0 87.4 all-gather.16
  536.0 9.2 reduce-scatter.4
where the time goes:
time: 558 us; the launch traced here: 556 us
  waiting for transfers between devices  453 us (81%)
  matrix products  48.4 us (9%)
  local copies, waits for them, and re-layouts  18 us (3%)
  other arithmetic  15.9 us (3%)
  between operations  13.7 us (2%)
  loops' own time  6.39 us (1%)
    all_gather x1, waiting for transfers between devices, on_device(): down_rows = lax.all_gather(down_weight, 'sp', axis=0, tiled=True)  90.1 us
    all_gather x1, waiting for transfers between devices, on_device(): lax.all_gather(gate_weight, 'sp', axis=0, tiled=True)  85.3 us
    all_gather x1, waiting for transfers between devices, on_device(): lax.all_gather(up_weight, 'sp', axis=0, tiled=True)  84.4 us
    all_gather x1, waiting for transfers between devices, on_device(): value_piece = lax.all_gather(values, 'sp', axis=0, tiled=True)  83.9 us
    all_gather x1, waiting for transfers between devices, on_device(): key_piece = lax.all_gather(keys, 'sp', axis=0, tiled=True)  71 us
    dot_general x7, matrix products, update(): jnp.einsum('hcrn,nhe->hcre', weights.astype(jnp.bfloat16), value_block, p...  18 us
    reduce_scatter x1, waiting for transfers between devices, on_device(): lax.psum_scatter(rounded(jnp.dot(section, out_weight, preferred_element_t...  15 us
    dot_general x7, matrix products, update(): jnp.einsum('rhcd,nhcd->hcrn', query_grid, key_block, preferred_element_ty...  13.3 us
  transfers between devices with their start and end apart: 8, of which 8 were waited for; matrix products, arithmetic and copies ran while one was open for 3% of the time, Pallas kernels for 0%

commit v1 on v0

--- a/solution.py
+++ b/solution.py
@@ -1,8 +1,11 @@
+import functools
 import math
 
 import jax
 import jax.numpy as jnp
 from jax import lax
+from jax.experimental import pallas as pl
+from jax.experimental.pallas import tpu as pltpu
 from jax.sharding import PartitionSpec as P
 
 KD = 64
@@ -141,6 +144,392 @@
     return (mixed.astype(jnp.float32) + normalize(ffn_out, ffn_gain)).astype(jnp.bfloat16)
 
 
+MESH = pl.DeviceIdType.MESH
+QUAD = 4
+F32 = jnp.float32
+BF16 = jnp.bfloat16
+
+
+def nt_dot(a, b):
+    return lax.dot_general(a, b, (((1,), (1,)), ((), ())), preferred_element_type=F32)
+
+
+def tn_dot(a, b):
+    return lax.dot_general(a, b, (((0,), (0,)), ((), ())), preferred_element_type=F32)
+
+
+def rms(matrix):
+    return matrix * lax.rsqrt(jnp.mean(matrix * matrix, axis=-1, keepdims=True) + epsilon)
+
+
+def layer_kernel(
+    q_ref, k_ref, v_ref, lam_ref, hgain_ref, ow_ref, res_ref, mgain_ref, pgain_ref,
+    gw_ref, uw_ref, dw_ref, fgain_ref, out_ref,
+    qbuf, kbuf, vbuf, gbuf, ubuf, dbuf, qz, m_st, l_st, acc_st, hs, ho,
+    ptx, prx, mixed, xbuf, pbuf, ftx, frx, fown, rtx, rrx,
+    send, recv, local,
+):
+    rows = q_ref.shape[0]
+    half = rows // 2
+    wrows = gw_ref.shape[0]
+    width = gbuf.shape[1]
+    lanes = 128
+    blocks = gw_ref.shape[1] // lanes
+    per = width // lanes
+    s = lax.axis_index("sp")
+    c = lax.axis_index("tp")
+    k = s // 8
+    q = (s // 2) % 4
+    x = s % 2
+    zl, y = q // 2, q % 2
+
+    def peer(d):
+        return (zl if d < 2 else 1 - zl) * 2 + (y if d % 2 == 0 else 1 - y)
+
+    def chip(kk, qq, xx):
+        return kk * 8 + qq * 2 + xx
+
+    sib = 1 - c
+    qs = [peer(d) for d in range(4)]
+    quad_dev = [(chip(k, qs[d], x), c) for d in range(4)]
+    x_dev = (chip(k, q, 1 - x), c)
+    k_dev = (chip(1 - k, q, x), c)
+    sib_dev = (s, sib)
+
+    barrier = pltpu.get_barrier_semaphore()
+    partners = quad_dev[1:] + [x_dev, k_dev, sib_dev]
+    for dev in partners:
+        pl.semaphore_signal(barrier, inc=1, device_id=dev, device_id_type=MESH)
+    pl.semaphore_wait(barrier, len(partners))
+
+    def rc(src, dst, i, dev):
+        return pltpu.make_async_remote_copy(
+            src_ref=src, dst_ref=dst, send_sem=send.at[i], recv_sem=recv.at[i],
+            device_id=dev, device_id_type=MESH,
+        )
+
+    def head_cols(qq):
+        return pl.ds(pl.multiple_of(qq * lanes, lanes), lanes)
+
+    def unit_start(qq):
+        return jnp.minimum(qq * per, blocks - per)
+
+    def unit_cols(qq):
+        return pl.ds(pl.multiple_of(unit_start(qq) * lanes, lanes), width)
+
+    def kv_rows(ss):
+        return pl.ds(pl.multiple_of(ss * rows, rows), rows)
+
+    def w_rows(ss):
+        return pl.ds(pl.multiple_of(ss * wrows, wrows), wrows)
+
+    started = []
+
+    def go(copy):
+        copy.start()
+        started.append(copy)
+
+    me = s
+    kv = [kbuf, vbuf]
+    ws = [gbuf, ubuf, dbuf]
+    own = []
+    for i, (src, dst, at, cols) in enumerate(
+        [
+            (q_ref, qbuf, kv_rows(q), head_cols(q)),
+            (k_ref, kbuf, kv_rows(me), head_cols(q)),
+            (v_ref, vbuf, kv_rows(me), head_cols(q)),
+            (gw_ref, gbuf, w_rows(me), unit_cols(q)),
+            (uw_ref, ubuf, w_rows(me), unit_cols(q)),
+            (dw_ref, dbuf, w_rows(me), unit_cols(q)),
+        ]
+    ):
+        cp = pltpu.make_async_copy(src.at[:, cols], dst.at[at, :], local.at[i])
+        cp.start()
+        own.append(cp)
+    for d in (1, 2, 3):
+        for a, (src, dst) in enumerate([(k_ref, kbuf), (v_ref, vbuf), (q_ref, qbuf)]):
+            slot = dst.at[kv_rows(me if a < 2 else q), :]
+            go(rc(src.at[:, head_cols(qs[d])], slot, (d - 1) * 6 + a, quad_dev[d]))
+    for d in (1, 2, 3):
+        for a, (src, dst) in enumerate([(gw_ref, gbuf), (uw_ref, ubuf), (dw_ref, dbuf)]):
+            go(rc(src.at[:, unit_cols(qs[d])], dst.at[w_rows(me), :], (d - 1) * 6 + 3 + a, quad_dev[d]))
+    for cp in own:
+        cp.wait()
+
+    X0, K0, R0 = 18, 38, 58
+    kv_cond = []
+
+    def kslot(a, ss):
+        return kv[a].at[kv_rows(ss), :]
+
+    def wslot(a, ss):
+        return ws[a].at[w_rows(ss), :]
+
+    for d in range(4):
+        ss = chip(k, qs[d], x)
+        for a in range(2):
+            slot = kslot(a, ss)
+            if d > 0:
+                rc(slot, slot, (d - 1) * 6 + a, quad_dev[d]).wait_recv()
+            go(rc(slot, slot, X0 + d * 5 + a, x_dev))
+            copy = rc(slot, slot, K0 + d * 5 + a, k_dev)
+            kv_cond.append(copy)
+
+            @pl.when(k == 0)
+            def _(copy=copy):
+                copy.start()
+
+    for d in range(4):
+        ss = chip(k, qs[d], x)
+        for a in range(3):
+            slot = wslot(a, ss)
+            if d > 0:
+                rc(slot, slot, (d - 1) * 6 + 3 + a, quad_dev[d]).wait_recv()
+            go(rc(slot, slot, K0 + d * 5 + 2 + a, k_dev))
+            go(rc(slot, slot, X0 + d * 5 + 2 + a, x_dev))
+    for d in (1, 2, 3):
+        slot = qbuf.at[kv_rows(qs[d]), :]
+        rc(slot, slot, (d - 1) * 6 + 2, quad_dev[d]).wait_recv()
+    for d in range(4):
+        for a in range(2):
+            slot = kslot(a, chip(k, qs[d], 1 - x))
+            rc(slot, slot, X0 + d * 5 + a, x_dev).wait_recv()
+
+    span = 2 * rows
+    lane = lax.broadcasted_iota(jnp.int32, (rows, lanes), 1)
+    for j in range(4):
+        piece = qbuf[j * rows : (j + 1) * rows, :].astype(F32) * (1.0 / math.sqrt(KD))
+        qz[j, :rows, :] = jnp.where(lane < KD, piece, 0.0).astype(BF16)
+        qz[j, rows:, :] = jnp.where(lane < KD, 0.0, piece).astype(BF16)
+
+    def pair_rows(p):
+        return pl.ds(pl.multiple_of(p * span, span), span)
+
+    def update(j, p, carry):
+        m, l, acc = carry
+        sc = nt_dot(kbuf[pair_rows(p), :], qz[j])
+        new = jnp.maximum(m, jnp.max(sc, axis=0, keepdims=True))
+        e = jnp.exp(sc - new)
+        f = jnp.exp(m - new)
+        l = l * f + jnp.sum(e, axis=0, keepdims=True)
+        acc = acc * f + tn_dot(vbuf[pair_rows(p), :], e.astype(BF16))
+        return new, l, acc
+
+    def chunk_a(j, _):
+        p = 4 * k + j
+        sc = nt_dot(kbuf[pair_rows(p), :], qz[j])
+        key_pos = lax.broadcasted_iota(jnp.int32, sc.shape, 0)
+        query_pos = x * rows + lax.broadcasted_iota(jnp.int32, sc.shape, 1) % rows
+        sc = jnp.where(key_pos <= query_pos, sc, negative)
+        m = jnp.max(sc, axis=0, keepdims=True)
+        e = jnp.exp(sc - m)
+        l = jnp.sum(e, axis=0, keepdims=True)
+        acc = tn_dot(vbuf[pair_rows(p), :], e.astype(BF16))
+        m, l, acc = lax.fori_loop(0, j, lambda i, carry: update(j, 4 * k + i, carry), (m, l, acc))
+        m_st[j], l_st[j], acc_st[j] = m, l, acc
+        return 0
+
+    lax.fori_loop(0, 4, chunk_a, 0)
+
+    relays = []
+    for d in range(4):
+        for a in range(2):
+            slot = kslot(a, chip(1 - k, qs[d], x))
+            relays.append(rc(slot, slot, R0 + d * 5 + a, x_dev))
+
+    @pl.when(k == 1)
+    def _():
+        for d in range(4):
+            for a in range(2):
+                slot = kslot(a, chip(1 - k, qs[d], x))
+                rc(slot, slot, K0 + d * 5 + a, k_dev).wait_recv()
+                relays[d * 2 + a].start()
+        for d in range(4):
+            for a in range(2):
+                slot = kslot(a, chip(1 - k, qs[d], 1 - x))
+                rc(slot, slot, R0 + d * 5 + a, x_dev).wait_recv()
+
+        def chunk_b(j, _):
+            carry = lax.fori_loop(
+                0, 4, lambda i, carry: update(j, i, carry), (m_st[j], l_st[j], acc_st[j])
+            )
+            m_st[j], l_st[j], acc_st[j] = carry
+            return 0
+
+        lax.fori_loop(0, 4, chunk_b, 0)
+
+    lam = lam_ref[q]
+
+    def finish(j, _):
+        ratio = acc_st[j] / l_st[j]
+        att = (ratio[:, :rows] - lam * ratio[:, rows:]).T
+        hs[j] = (rms(att) * hgain_ref[...]).astype(BF16)
+        return 0
+
+    lax.fori_loop(0, 4, finish, 0)
+    H0 = 78
+    for d in (3, 1, 2):
+        go(rc(hs.at[qs[d]], ho.at[q], H0 + d - 1, quad_dev[d]))
+    ho[q] = hs[q]
+    for d in (1, 2, 3):
+        rc(ho.at[qs[d]], ho.at[qs[d]], H0 + d - 1, quad_dev[d]).wait_recv()
+
+    def head_rows(cc):
+        at = pl.ds(pl.multiple_of(cc * half, half), half)
+        return jnp.concatenate([ho[j, at, :] for j in range(4)], axis=1)
+
+    theirs = head_rows(sib)
+    ptx[...] = jnp.dot(theirs, ow_ref[...], preferred_element_type=F32).astype(BF16)
+    P0 = 81
+    go(rc(ptx, prx, P0, sib_dev))
+    mixed[...] = jnp.dot(head_rows(c), ow_ref[...], preferred_element_type=F32)
+    rc(prx, prx, P0, sib_dev).wait_recv()
+
+    strip = 16
+
+    def mix(i, _):
+        at = pl.ds(pl.multiple_of(i * strip, strip), strip)
+        total = mixed[at, :].astype(BF16).astype(F32) + prx[at, :].astype(F32)
+        mx = (res_ref[at, :].astype(F32) + rms(total) * mgain_ref[...]).astype(BF16).astype(F32)
+        mixed[at, :] = mx
+        xbuf[q, pl.ds(pl.multiple_of(c * half + i * strip, strip), strip), :] = (
+            rms(mx) * pgain_ref[...]
+        ).astype(BF16)
+        return 0
+
+    lax.fori_loop(0, half // strip, mix, 0)
+
+    A0, S0 = 82, 85
+    core_rows = [pl.ds(pl.multiple_of(cc * half, half), half) for cc in (c, sib)]
+    mine = xbuf.at[q, core_rows[0], :]
+    for d in (3, 1, 2):
+        go(rc(mine, mine, A0 + d - 1, quad_dev[d]))
+    go(rc(mine, mine, S0, sib_dev))
+
+    for d in range(4):
+        for a in range(3):
+            slot = wslot(a, chip(1 - k, qs[d], x))
+            rc(slot, slot, K0 + d * 5 + 2 + a, k_dev).wait_recv()
+            go(rc(slot, slot, R0 + d * 5 + 2 + a, x_dev))
+    for d in (1, 2, 3):
+        slot = xbuf.at[qs[d], core_rows[0], :]
+        rc(slot, slot, A0 + d - 1, quad_dev[d]).wait_recv()
+        go(rc(slot, slot, S0 + d, sib_dev))
+    for a in range(3):
+        for d in range(4):
+            slot = wslot(a, chip(k, qs[d], 1 - x))
+            rc(slot, slot, X0 + d * 5 + 2 + a, x_dev).wait_recv()
+        for d in range(4):
+            slot = wslot(a, chip(1 - k, qs[d], 1 - x))
+            rc(slot, slot, R0 + d * 5 + 2 + a, x_dev).wait_recv()
+
+    F0, C0 = 89, 93
+    fresh = (q * per - unit_start(q)) * lanes
+    unit = lax.broadcasted_iota(jnp.int32, (rows, width), 1)
+
+    def summed(d):
+        slot = frx.at[d]
+        rc(slot, slot, F0 + d, sib_dev).wait_recv()
+        total = fown[d].astype(F32) + frx[d].astype(F32)
+        if d == 0:
+            fown[0] = total.astype(BF16)
+        else:
+            rtx[d - 1] = total.astype(BF16)
+            go(rc(rtx.at[d - 1], rrx.at[d - 1], C0 + d - 1, quad_dev[d]))
+
+    order = (3, 1, 2, 0)
+    for n, d in enumerate(order):
+        slot = xbuf.at[qs[d], core_rows[1], :]
+        rc(slot, slot, S0 + d, sib_dev).wait_recv()
+        rows_in = xbuf[qs[d]]
+        gate = jnp.dot(rows_in, gbuf[...], preferred_element_type=F32)
+        up = jnp.dot(rows_in, ubuf[...], preferred_element_type=F32)
+        hid = gate / (1.0 + jnp.exp(-gate)) * up
+        hid = jnp.where(unit >= fresh, hid, 0.0).astype(BF16)
+        pbuf[...] = nt_dot(hid, dbuf[...]).astype(BF16)
+        ftx[d] = pbuf[core_rows[1], :]
+        fown[d] = pbuf[core_rows[0], :]
+        go(rc(ftx.at[d], frx.at[d], F0 + d, sib_dev))
+        if n > 0:
+            summed(order[n - 1])
+    summed(order[-1])
+    for d in (1, 2, 3):
+        slot = rrx.at[d - 1]
+        rc(slot, slot, C0 + d - 1, quad_dev[d]).wait_recv()
+
+    def last(i, _):
+        at = pl.ds(pl.multiple_of(i * strip, strip), strip)
+        total = fown[0, at, :].astype(F32)
+        for d in range(3):
+            total = total + rrx[d, at, :].astype(F32)
+        out_ref[at, :] = (mixed[at, :] + rms(total) * fgain_ref[...]).astype(BF16)
+        return 0
+
+    lax.fori_loop(0, half // strip, last, 0)
+
+    for copy in started:
+        copy.wait_send()
+
+    @pl.when(k == 0)
+    def _():
+        for copy in kv_cond:
+            copy.wait_send()
+
+    @pl.when(k == 1)
+    def _():
+        for copy in relays:
+            copy.wait_send()
+
+
+def fused(sp, queries, keys, values, lambdas, head_gain, out_weight, residual, mix_gain,
+          pre_gain, gate_weight, up_weight, down_weight, ffn_gain):
+    rows, width = queries.shape[0], 128 * -(-(gate_weight.shape[1] // 128) // QUAD)
+    half, model = residual.shape
+    wrows = gate_weight.shape[0]
+    vm = pl.BlockSpec(memory_space=pltpu.VMEM)
+    V = pltpu.VMEM
+    return pl.pallas_call(
+        layer_kernel,
+        out_shape=jax.ShapeDtypeStruct((half, model), BF16),
+        in_specs=[vm, vm, vm, pl.BlockSpec(memory_space=pltpu.SMEM)] + [vm] * 9,
+        out_specs=vm,
+        scratch_shapes=[
+            V((QUAD * rows, VD), BF16),
+            V((sp * rows, VD), BF16),
+            V((sp * rows, VD), BF16),
+            V((sp * wrows, width), BF16),
+            V((sp * wrows, width), BF16),
+            V((sp * wrows, width), BF16),
+            V((QUAD, 2 * rows, VD), BF16),
+            V((QUAD, 1, 2 * rows), F32),
+            V((QUAD, 1, 2 * rows), F32),
+            V((QUAD, VD, 2 * rows), F32),
+            V((QUAD, rows, VD), BF16),
+            V((QUAD, rows, VD), BF16),
+            V((half, model), BF16),
+            V((half, model), BF16),
+            V((half, model), F32),
+            V((QUAD, rows, model), BF16),
+            V((rows, model), BF16),
+            V((QUAD, half, model), BF16),
+            V((QUAD, half, model), BF16),
+            V((QUAD, half, model), BF16),
+            V((QUAD - 1, half, model), BF16),
+            V((QUAD - 1, half, model), BF16),
+            pltpu.SemaphoreType.DMA((96,)),
+            pltpu.SemaphoreType.DMA((96,)),
+            pltpu.SemaphoreType.DMA((6,)),
+        ],
+        compiler_params=pltpu.CompilerParams(
+            collective_id=0, has_side_effects=True, vmem_limit_bytes=60 * 1024 * 1024
+        ),
+    )(
+        queries, keys, values, lambdas, head_gain[None, :], out_weight, residual,
+        mix_gain[None, :], pre_gain[None, :], gate_weight, up_weight, down_weight,
+        ffn_gain[None, :],
+    )
+
+
 def solution(mesh):
     in_specs = (
         P("sp", "tp"),
@@ -158,6 +547,8 @@
         P(),
     )
     out_specs = P(("sp", "tp"), None)
+    sp, tp = mesh.shape["sp"], mesh.shape["tp"]
+    body = functools.partial(fused, sp) if (sp, tp) == (16, 2) else on_device
     return jax.shard_map(
-        on_device, mesh=mesh, in_specs=in_specs, out_specs=out_specs, check_vma=False
+        body, mesh=mesh, in_specs=in_specs, out_specs=out_specs, check_vma=False
     )

time: 558 us -> 155 us (0.28)
  waiting for transfers between devices: 453 us -> 0 us
  Pallas kernels: 0 us -> 153 us
  matrix products: 48.4 us -> 0 us
  local copies, waits for them, and re-layouts: 18 us -> 1.88 us
  other arithmetic: 15.9 us -> 0 us
  between operations: 13.7 us -> 0.01 us
  loops' own time: 6.39 us -> 0 us
    all_gather x6 -> x0, waiting for transfers between devices: 426 us -> none  [the longest x1 90.1 us: on_device(): down_rows = lax.all_gather(down_weight, 'sp', axis=0, tiled=True)]
    pallas_call x0 -> x1, Pallas kernels: none -> 153 us  [fused(): pl.pallas_call(layer_kernel, out_shape=jax.ShapeDtypeStruct((half, model)...]
    dot_general x17 -> x0, matrix products: 48.4 us -> none  [the longest x7 18 us: update(): jnp.einsum('hcrn,nhe->hcre', weights.astype(jnp.bfloat16), value_block, p...]
    reduce_scatter x2 -> x0, waiting for transfers between devices: 24.4 us -> none  [the longest x1 15 us: on_device(): lax.psum_scatter(rounded(jnp.dot(section, out_weight, preferred_element_t...]
    reduce_sum x11 -> x0, other arithmetic: 10.2 us -> none  [the longest x7 6.1 us: update(): totals = totals * factor + jnp.sum(weights, axis=-1)]
    unnamed x17 -> x1, local copies, waits for them, and re-layouts: 9.41 us -> 1.88 us
    all_gather x1 -> x0, local copies, waits for them, and re-layouts: 6.5 us -> none  [on_device(): key_piece = lax.all_gather(keys, 'sp', axis=0, tiled=True)]
    another operation x9 -> x0, loops' own time: 6.39 us -> none  [the longest x1 5.81 us: on_device(): results.append(lax.fori_loop(0, count // block, visit, carried_group))]
  transfers between devices with their start and end apart: 8 -> 0, of which waited for: 8 -> 0; matrix products, arithmetic and copies ran while one was open for 3% -> 0% of each run, Pallas kernels for 0% -> 0%
where the time goes in v1:
time: 155 us
  Pallas kernels  153 us (99%)
  local copies, waits for them, and re-layouts  1.88 us (1%)
    pallas_call x1, Pallas kernels, fused(): pl.pallas_call(layer_kernel, out_shape=jax.ShapeDtypeStruct((half, model)...  153 us

profile of v1, /device:TPU:25, one launch (start us, length us, event | category | flops | bytes accessed | tf_op | source)
XLA Modules:
  0.0 155.3 jit_solution(8675420897085247357)
XLA Ops:
  0.0 153.4 %shard_map.127 = bf16[128,2048]{1,0:T(8,128)(2,1)} custom-call(bf16[256,512]{1,0:T(8,128)(2,1)} %q_ref.1, bf16[256,512]{1,0:T(8,128)(2,1)} %k_ref.1, bf16[256,512]{1,0:T(8,128)(2,1)} %v_ref.1, f32[4]{0:T(128)} %lam_ref.1, f32[1,128]{1,0:T(1,128)} %bitcast.7, bf16[512,2048]{1,0:T(8,128)(2,1)} %ow_ref.1, bf16[128,2048]{1,0:T(8,128)(2,1)} %res_ref.1, ...), custom_call_target="tpu_custom_call" | custom-call | tf_op jit(solution)/shard_map/pallas_call | solution.py:491
  153.4 1.9 %copy.15 = bf16[128,2048]{1,0:T(8,128)(2,1)} copy(bf16[128,2048]{1,0:T(8,128)(2,1)} %shard_map.127) | data formatting | bytes 1048576

commit v2 on v1

--- a/solution.py
+++ b/solution.py
@@ -165,29 +165,37 @@
 def layer_kernel(
     q_ref, k_ref, v_ref, lam_ref, hgain_ref, ow_ref, res_ref, mgain_ref, pgain_ref,
     gw_ref, uw_ref, dw_ref, fgain_ref, out_ref,
-    qbuf, kbuf, vbuf, gbuf, ubuf, dbuf, qz, m_st, l_st, acc_st, hs, ho,
+    qbuf, kvbuf, wbuf, qz, m_st, l_st, acc_st, hs, ho,
     ptx, prx, mixed, xbuf, pbuf, ftx, frx, fown, rtx, rrx,
     send, recv, local,
 ):
     rows = q_ref.shape[0]
     half = rows // 2
     wrows = gw_ref.shape[0]
-    width = gbuf.shape[1]
+    width = wbuf.shape[1] // 3
+    kbuf, vbuf = (kvbuf.at[:, i * VD : (i + 1) * VD] for i in range(2))
+    gbuf, ubuf, dbuf = (wbuf.at[:, i * width : (i + 1) * width] for i in range(3))
     lanes = 128
     blocks = gw_ref.shape[1] // lanes
     per = width // lanes
     s = lax.axis_index("sp")
     c = lax.axis_index("tp")
     k = s // 8
-    q = (s // 2) % 4
     x = s % 2
-    zl, y = q // 2, q % 2
+    y = (s // 2) % 2
+
+    def place(kk, qq):
+        zz = qq // 2
+        return (zz + kk * (1 - 2 * zz)) * 2 + qq % 2
+
+    q = place(k, (s // 2) % 4)
+    zl = q // 2
 
     def peer(d):
         return (zl if d < 2 else 1 - zl) * 2 + (y if d % 2 == 0 else 1 - y)
 
     def chip(kk, qq, xx):
-        return kk * 8 + qq * 2 + xx
+        return kk * 8 + place(kk, qq) * 2 + xx
 
     sib = 1 - c
     qs = [peer(d) for d in range(4)]
@@ -235,7 +243,7 @@
     own = []
     for i, (src, dst, at, cols) in enumerate(
         [
-            (q_ref, qbuf, kv_rows(q), head_cols(q)),
+            (q_ref, qbuf, kv_rows(place(k, q)), head_cols(q)),
             (k_ref, kbuf, kv_rows(me), head_cols(q)),
             (v_ref, vbuf, kv_rows(me), head_cols(q)),
             (gw_ref, gbuf, w_rows(me), unit_cols(q)),
@@ -248,7 +256,7 @@
         own.append(cp)
     for d in (1, 2, 3):
         for a, (src, dst) in enumerate([(k_ref, kbuf), (v_ref, vbuf), (q_ref, qbuf)]):
-            slot = dst.at[kv_rows(me if a < 2 else q), :]
+            slot = dst.at[kv_rows(me if a < 2 else place(k, q)), :]
             go(rc(src.at[:, head_cols(qs[d])], slot, (d - 1) * 6 + a, quad_dev[d]))
     for d in (1, 2, 3):
         for a, (src, dst) in enumerate([(gw_ref, gbuf), (uw_ref, ubuf), (dw_ref, dbuf)]):
@@ -259,40 +267,56 @@
     X0, K0, R0 = 18, 38, 58
     kv_cond = []
 
+    def kvslot(ss):
+        return kvbuf.at[kv_rows(ss), :]
+
+    def allslot(ss):
+        return wbuf.at[w_rows(ss), :]
+
     def kslot(a, ss):
         return kv[a].at[kv_rows(ss), :]
 
     def wslot(a, ss):
         return ws[a].at[w_rows(ss), :]
 
-    for d in range(4):
+    def forward_kv(d):
         ss = chip(k, qs[d], x)
-        for a in range(2):
-            slot = kslot(a, ss)
-            if d > 0:
+        if d > 0:
+            for a in range(2):
+                slot = kslot(a, ss)
                 rc(slot, slot, (d - 1) * 6 + a, quad_dev[d]).wait_recv()
-            go(rc(slot, slot, X0 + d * 5 + a, x_dev))
-            copy = rc(slot, slot, K0 + d * 5 + a, k_dev)
-            kv_cond.append(copy)
-
-            @pl.when(k == 0)
-            def _(copy=copy):
-                copy.start()
-
-    for d in range(4):
+        slot = kvslot(ss)
+        copy = rc(slot, slot, K0 + d * 5, k_dev)
+        kv_cond.append(copy)
+
+        @pl.when(k == 0)
+        def _(copy=copy):
+            copy.start()
+
+        go(rc(slot, slot, X0 + d * 5, x_dev))
+
+    def forward_w(d):
         ss = chip(k, qs[d], x)
-        for a in range(3):
-            slot = wslot(a, ss)
-            if d > 0:
+        if d > 0:
+            for a in range(3):
+                slot = wslot(a, ss)
                 rc(slot, slot, (d - 1) * 6 + 3 + a, quad_dev[d]).wait_recv()
-            go(rc(slot, slot, K0 + d * 5 + 2 + a, k_dev))
-            go(rc(slot, slot, X0 + d * 5 + 2 + a, x_dev))
-    for d in (1, 2, 3):
-        slot = qbuf.at[kv_rows(qs[d]), :]
+        slot = allslot(ss)
+        go(rc(slot, slot, K0 + d * 5 + 2, k_dev))
+        go(rc(slot, slot, X0 + d * 5 + 2, x_dev))
+
+    forward_kv(0)
+    forward_w(0)
+    for d in (1, 2, 3):
+        forward_kv(d)
+    for d in (1, 2, 3):
+        forward_w(d)
+    for d in (1, 2, 3):
+        slot = qbuf.at[kv_rows(place(k, qs[d])), :]
         rc(slot, slot, (d - 1) * 6 + 2, quad_dev[d]).wait_recv()
     for d in range(4):
-        for a in range(2):
-            slot = kslot(a, chip(k, qs[d], 1 - x))
+        for a in range(1):
+            slot = kvslot(chip(k, qs[d], 1 - x))
             rc(slot, slot, X0 + d * 5 + a, x_dev).wait_recv()
 
     span = 2 * rows
@@ -329,34 +353,43 @@
         m_st[j], l_st[j], acc_st[j] = m, l, acc
         return 0
 
-    lax.fori_loop(0, 4, chunk_a, 0)
-
     relays = []
     for d in range(4):
-        for a in range(2):
-            slot = kslot(a, chip(1 - k, qs[d], x))
+        for a in range(1):
+            slot = kvslot(chip(1 - k, qs[d], x))
             relays.append(rc(slot, slot, R0 + d * 5 + a, x_dev))
 
-    @pl.when(k == 1)
-    def _():
-        for d in range(4):
-            for a in range(2):
-                slot = kslot(a, chip(1 - k, qs[d], x))
+    def relay_kv(d):
+        @pl.when(k == 1)
+        def _():
+            for a in range(1):
+                slot = kvslot(chip(1 - k, qs[d], x))
                 rc(slot, slot, K0 + d * 5 + a, k_dev).wait_recv()
-                relays[d * 2 + a].start()
-        for d in range(4):
-            for a in range(2):
-                slot = kslot(a, chip(1 - k, qs[d], 1 - x))
+                relays[d].start()
+
+    def chunk_b(d):
+        @pl.when(k == 1)
+        def _():
+            for a in range(1):
+                slot = kvslot(chip(1 - k, qs[d], 1 - x))
                 rc(slot, slot, R0 + d * 5 + a, x_dev).wait_recv()
 
-        def chunk_b(j, _):
-            carry = lax.fori_loop(
-                0, 4, lambda i, carry: update(j, i, carry), (m_st[j], l_st[j], acc_st[j])
-            )
-            m_st[j], l_st[j], acc_st[j] = carry
-            return 0
-
-        lax.fori_loop(0, 4, chunk_b, 0)
+            def one(j, _):
+                m_st[j], l_st[j], acc_st[j] = update(j, qs[d], (m_st[j], l_st[j], acc_st[j]))
+                return 0
+
+            lax.fori_loop(0, 4, one, 0)
+
+    lax.fori_loop(0, 3, chunk_a, 0)
+    relay_kv(0)
+    lax.fori_loop(3, 4, chunk_a, 0)
+    relay_kv(1)
+    chunk_b(0)
+    relay_kv(2)
+    chunk_b(1)
+    relay_kv(3)
+    chunk_b(2)
+    chunk_b(3)
 
     lam = lam_ref[q]
 
@@ -369,8 +402,16 @@
     lax.fori_loop(0, 4, finish, 0)
     H0 = 78
     for d in (3, 1, 2):
-        go(rc(hs.at[qs[d]], ho.at[q], H0 + d - 1, quad_dev[d]))
-    ho[q] = hs[q]
+        go(rc(hs.at[place(k, qs[d])], ho.at[q], H0 + d - 1, quad_dev[d]))
+    ho[q] = hs[place(k, q)]
+
+    def relay_w(d):
+        for a in range(1):
+            slot = allslot(chip(1 - k, qs[d], x))
+            rc(slot, slot, K0 + d * 5 + 2 + a, k_dev).wait_recv()
+            go(rc(slot, slot, R0 + d * 5 + 2 + a, x_dev))
+
+    relay_w(0)
     for d in (1, 2, 3):
         rc(ho.at[qs[d]], ho.at[qs[d]], H0 + d - 1, quad_dev[d]).wait_recv()
 
@@ -382,10 +423,16 @@
     ptx[...] = jnp.dot(theirs, ow_ref[...], preferred_element_type=F32).astype(BF16)
     P0 = 81
     go(rc(ptx, prx, P0, sib_dev))
+    relay_w(1)
     mixed[...] = jnp.dot(head_rows(c), ow_ref[...], preferred_element_type=F32)
     rc(prx, prx, P0, sib_dev).wait_recv()
 
     strip = 16
+
+    def pass_rows(d):
+        slot = xbuf.at[qs[d], core_rows[0], :]
+        rc(slot, slot, A0 + d - 1, quad_dev[d]).wait_recv()
+        go(rc(slot, slot, S0 + d, sib_dev))
 
     def mix(i, _):
         at = pl.ds(pl.multiple_of(i * strip, strip), strip)
@@ -406,21 +453,16 @@
         go(rc(mine, mine, A0 + d - 1, quad_dev[d]))
     go(rc(mine, mine, S0, sib_dev))
 
-    for d in range(4):
-        for a in range(3):
-            slot = wslot(a, chip(1 - k, qs[d], x))
-            rc(slot, slot, K0 + d * 5 + 2 + a, k_dev).wait_recv()
-            go(rc(slot, slot, R0 + d * 5 + 2 + a, x_dev))
-    for d in (1, 2, 3):
-        slot = xbuf.at[qs[d], core_rows[0], :]
-        rc(slot, slot, A0 + d - 1, quad_dev[d]).wait_recv()
-        go(rc(slot, slot, S0 + d, sib_dev))
-    for a in range(3):
+    for d in (1, 2):
+        relay_w(d + 1)
+        pass_rows(d)
+    pass_rows(3)
+    for a in range(1):
         for d in range(4):
-            slot = wslot(a, chip(k, qs[d], 1 - x))
+            slot = allslot(chip(k, qs[d], 1 - x))
             rc(slot, slot, X0 + d * 5 + 2 + a, x_dev).wait_recv()
         for d in range(4):
-            slot = wslot(a, chip(1 - k, qs[d], 1 - x))
+            slot = allslot(chip(1 - k, qs[d], 1 - x))
             rc(slot, slot, R0 + d * 5 + 2 + a, x_dev).wait_recv()
 
     F0, C0 = 89, 93
@@ -495,11 +537,8 @@
         out_specs=vm,
         scratch_shapes=[
             V((QUAD * rows, VD), BF16),
-            V((sp * rows, VD), BF16),
-            V((sp * rows, VD), BF16),
-            V((sp * wrows, width), BF16),
-            V((sp * wrows, width), BF16),
-            V((sp * wrows, width), BF16),
+            V((sp * rows, 2 * VD), BF16),
+            V((sp * wrows, 3 * width), BF16),
             V((QUAD, 2 * rows, VD), BF16),
             V((QUAD, 1, 2 * rows), F32),
             V((QUAD, 1, 2 * rows), F32),

time: 155 us -> 137 us (0.88); the launches traced: 155 us -> 136 us
  Pallas kernels: 153 us -> 134 us
    pallas_call x1, Pallas kernels: 153 us -> 134 us  [fused(): pl.pallas_call(layer_kernel, out_shape=jax.ShapeDtypeStruct((half, model)...]
where the time goes in v2:
time: 137 us; the launch traced here: 136 us
  Pallas kernels  134 us (98%)
  local copies, waits for them, and re-layouts  1.88 us (1%)
    pallas_call x1, Pallas kernels, fused(): pl.pallas_call(layer_kernel, out_shape=jax.ShapeDtypeStruct((half, model)...  134 us

profile of v2, /device:TPU:25, one launch (start us, length us, event | category | flops | bytes accessed | tf_op | source)
XLA Modules:
  0.0 135.6 jit_solution(204584751207702045)
XLA Ops:
  0.0 133.7 %shard_map.127 = bf16[128,2048]{1,0:T(8,128)(2,1)} custom-call(bf16[256,512]{1,0:T(8,128)(2,1)} %q_ref.1, bf16[256,512]{1,0:T(8,128)(2,1)} %k_ref.1, bf16[256,512]{1,0:T(8,128)(2,1)} %v_ref.1, f32[4]{0:T(128)} %lam_ref.1, f32[1,128]{1,0:T(1,128)} %bitcast.7, bf16[512,2048]{1,0:T(8,128)(2,1)} %ow_ref.1, bf16[128,2048]{1,0:T(8,128)(2,1)} %res_ref.1, ...), custom_call_target="tpu_custom_call" | custom-call | tf_op jit(solution)/shard_map/pallas_call | solution.py:533
  133.8 1.9 %copy.15 = bf16[128,2048]{1,0:T(8,128)(2,1)} copy(bf16[128,2048]{1,0:T(8,128)(2,1)} %shard_map.127) | data formatting | bytes 1048576
